TPU v7x, 32 devices: a whole 2x2x4 slice. The times are simulated.
32 devices in a mesh: sp: 8 (over z, x), dp: 4 (over y, core).
Axes of the slice: x: 2, y: 2, z: 4, core: 2. Of those that a mesh axis runs over, the one named last changes fastest.
Arguments:
- resid: bfloat16 [4, 2048, 2048], P('dp', 'sp'), may hold values from -4 to 4
- query: bfloat16 [4, 2048, 2048], P('dp', 'sp'), may hold values from -6 to 6
- keys: bfloat16 [4, 2048, 512], P('dp', 'sp'), may hold values from -6 to 6
- values: bfloat16 [4, 2048, 512], P('dp', 'sp'), may hold values from -6 to 6
- q_gain: float32 [128], replicated, may hold values from 0.7 to 5
- k_gain: float32 [128], replicated, may hold values from 0.7 to 5
- out_weight: bfloat16 [2048, 2048], P('dp'), may hold values from -0.5 to 0.5
- norm_gain: float32 [2048], replicated, may hold values from 0.1 to 1.9
- route_ids: int32 [4, 2048, 2], P('dp', 'sp'), may hold values from 0 to 31, all different within a row; in each aligned block of 256 rows (0 to 255, 256 to 511, ..., all dimensions but the last counted through in order) at most 24 rows name the same one
- route_weight: float32 [4, 2048, 2], P('dp', 'sp'), may hold values from 0.2 to 1
- expert_gate: bfloat16 [32, 2048, 1024], P(('sp', 'dp')), may hold values from -0.125 to 0.125
- expert_up: bfloat16 [32, 2048, 1024], P(('sp', 'dp')), may hold values from -0.125 to 0.125
- expert_down: bfloat16 [32, 1024, 2048], P(('sp', 'dp')), may hold values from -0.1875 to 0.1875
Outputs:
- layer_out: bfloat16 [4, 2048, 2048], P('dp', 'sp')
Inputs may be any that keep to these rules, and one draw needn't show every extreme that they name: `route_ids`: each row names 2 different experts. In the rows of one device no expert is named more than 24 times, and in some devices some expert is named exactly 24 times.
All inputs are finite; a program needn't handle non-finite values.
Results may differ from a plain program's by a relative error of at most 0.0095.
The roundings to bfloat16 on the way count: a program that leaves them out, or rounds other values in their place, can miss the bound.
Values may be sent and summed in bfloat16 or wider, within the bound.
A program may use at most 128 MiB of HBM per device.

v0:
```python
import jax
import jax.numpy as jnp
from jax import lax
from jax.sharding import PartitionSpec as P

GRID_W = 64
EPSILON = 1e-06
THETA = 10000.0
LIMIT = 7.0
SLOPE = 1.702


def turn_half(matrix, places):
    half_width = matrix.shape[-1] // 2
    inverse = THETA ** (-jnp.arange(half_width, dtype=jnp.float32) / half_width)
    angles = places.astype(jnp.float32)[:, None] * inverse[None, :]
    cosine = jnp.cos(angles)[:, None, :]
    sine_part = jnp.sin(angles)[:, None, :]
    leading = matrix[..., :half_width]
    second = matrix[..., half_width:]
    return jnp.concatenate(
        [leading * cosine - second * sine_part, second * cosine + leading * sine_part], axis=-1
    )


def prepare(projected_rows, gain_vector, head_count, places):
    matrix = projected_rows.astype(jnp.float32).reshape(projected_rows.shape[0], head_count, -1)
    matrix = (
        matrix
        * lax.rsqrt(jnp.mean(matrix * matrix, axis=-1, keepdims=True) + EPSILON)
        * gain_vector
    )
    middle = matrix.shape[-1] // 2
    turned = jnp.concatenate(
        [
            turn_half(matrix[..., :middle], places // GRID_W),
            turn_half(matrix[..., middle:], places % GRID_W),
        ],
        axis=-1,
    )
    return turned.astype(jnp.bfloat16)


def attend(head_query, head_key, head_value):
    length, local_heads, head_dim = head_query.shape
    local_kv = head_key.shape[1]
    group_size = local_heads // local_kv
    block_rows = min(512, length)
    scaling = head_dim ** (-0.5)
    query_blocks = head_query.reshape(
        length // block_rows, block_rows, local_kv, group_size, head_dim
    )

    def one_block(query_block):
        scores = (
            jnp.einsum("qkgd,skd->kgqs", query_block, head_key, preferred_element_type=jnp.float32)
            * scaling
        )
        lifted = jnp.exp(scores - jnp.max(scores, axis=-1, keepdims=True))
        attn_weights = (lifted / jnp.sum(lifted, axis=-1, keepdims=True)).astype(jnp.bfloat16)
        return jnp.einsum(
            "kgqs,skd->qkgd", attn_weights, head_value, preferred_element_type=jnp.float32
        ).astype(jnp.bfloat16)

    return lax.map(one_block, query_blocks).reshape(length, local_heads, head_dim)


def apply_expert(batch, gate_matrix, up_matrix, down_matrix):
    flat_rows = batch.reshape(-1, batch.shape[-1])
    gated = jnp.minimum(jnp.dot(flat_rows, gate_matrix, preferred_element_type=jnp.float32), LIMIT)
    linear = jnp.clip(
        jnp.dot(flat_rows, up_matrix, preferred_element_type=jnp.float32), -LIMIT, LIMIT
    )
    active = (gated * jax.nn.sigmoid(SLOPE * gated) * (linear + 1.0)).astype(jnp.bfloat16)
    return (
        jnp.dot(active, down_matrix, preferred_element_type=jnp.float32)
        .astype(jnp.bfloat16)
        .reshape(batch.shape)
    )


def per_device(
    resid,
    query,
    keys,
    values,
    q_gain,
    k_gain,
    out_weight,
    norm_gain,
    route_ids,
    route_weight,
    expert_gate,
    expert_up,
    expert_down,
):
    span_devices = lax.axis_size("sp")
    experts_total = span_devices * lax.axis_size("dp")
    tok_rows = resid.shape[1]
    model_width = resid.shape[2]
    head_dim = q_gain.shape[0]
    q_heads = query.shape[2] // head_dim
    kv_heads = keys.shape[2] // head_dim
    repeat_count = max(kv_heads, span_devices) // kv_heads
    places = lax.axis_index("sp") * tok_rows + jnp.arange(tok_rows, dtype=jnp.int32)
    query_turned = prepare(query[0], q_gain, q_heads, places)
    key_turned = jnp.repeat(prepare(keys[0], k_gain, kv_heads, places), repeat_count, axis=1)
    value_heads = jnp.repeat(values[0].reshape(tok_rows, kv_heads, head_dim), repeat_count, axis=1)
    head_query, head_key, head_value = (
        lax.all_to_all(query_turned, "sp", split_axis=1, concat_axis=0, tiled=True),
        lax.all_to_all(key_turned, "sp", split_axis=1, concat_axis=0, tiled=True),
        lax.all_to_all(value_heads, "sp", split_axis=1, concat_axis=0, tiled=True),
    )
    head_out = attend(head_query, head_key, head_value)
    token_out = lax.all_to_all(head_out, "sp", split_axis=0, concat_axis=1, tiled=True).reshape(
        tok_rows, q_heads * head_dim
    )
    projected = jnp.dot(
        token_out,
        lax.all_gather(out_weight, "dp", axis=0, tiled=True),
        preferred_element_type=jnp.float32,
    )
    updated = (resid[0].astype(jnp.float32) + projected).astype(jnp.bfloat16)
    widened = updated.astype(jnp.float32)
    normed = (
        widened
        * lax.rsqrt(jnp.mean(widened * widened, axis=-1, keepdims=True) + EPSILON)
        * norm_gain
    ).astype(jnp.bfloat16)
    top_count = route_ids.shape[2]
    capacity = max(2, 3 * tok_rows * top_count // (2 * experts_total))
    chosen = route_ids[0].reshape(-1)
    onehot = (chosen[:, None] == jnp.arange(experts_total, dtype=jnp.int32)[None, :]).astype(
        jnp.int32
    )
    earlier = jnp.sum((jnp.cumsum(onehot, axis=0) - onehot) * onehot, axis=1)
    target = chosen * capacity + earlier
    sources = jnp.arange(tok_rows * top_count, dtype=jnp.int32) // top_count
    slot_table = jnp.full((experts_total * capacity,), tok_rows, jnp.int32).at[target].set(sources)
    padded = jnp.concatenate([normed, jnp.zeros((1, model_width), jnp.bfloat16)], axis=0)
    outgoing = padded[slot_table].reshape(experts_total, capacity, model_width)
    answered = apply_expert(
        lax.all_to_all(outgoing, ("sp", "dp"), split_axis=0, concat_axis=0, tiled=True),
        expert_gate[0],
        expert_up[0],
        expert_down[0],
    )
    returned = lax.all_to_all(answered, ("sp", "dp"), split_axis=0, concat_axis=0, tiled=True)
    results = returned.reshape(experts_total * capacity, model_width)[target]
    weighted = results.astype(jnp.float32) * route_weight[0].reshape(-1)[:, None]
    combined = jnp.sum(weighted.reshape(tok_rows, top_count, model_width), axis=1)
    return (widened + combined).astype(jnp.bfloat16)[None]


def solution(mesh):
    placed = (
        P("dp", "sp", None),
        P("dp", "sp", None),
        P("dp", "sp", None),
        P("dp", "sp", None),
        P(),
        P(),
        P("dp", None),
        P(),
        P("dp", "sp", None),
        P("dp", "sp", None),
        P(("sp", "dp"), None, None),
        P(("sp", "dp"), None, None),
        P(("sp", "dp"), None, None),
    )
    return jax.shard_map(
        per_device, mesh=mesh, in_specs=placed, out_specs=P("dp", "sp", None), check_vma=False
    )
```

profile of v0, /device:TPU:0, one launch (start us, length us, event | category | flops | bytes accessed | tf_op | source)
XLA Modules:
  0.0 339.7 jit_solution(17231066613141276203)
XLA Ops:
  12.4 7.3 %all-to-all-start.1 = ((bf16[256,8,128]{2,0,1:T(8,128)(2,1)}), bf16[256,8,128]{2,0,1:T(8,128)(2,1)S(1)}, u32[]{:S(2)}, u32[]{:S(2)}) async-start(bf16[256,8,128]{2,0,1:T(8,128)(2,1)} %bitcast.22), calls=%async_computation.1 | async-start | bytes 1048576 | tf_op jit(solution)/shard_map/all_to_all | solution.py:111
  22.3 11.9 %all-to-all-done.1 = bf16[256,8,128]{2,0,1:T(8,128)(2,1)S(1)} async-done(((bf16[256,8,128]{2,0,1:T(8,128)(2,1)}), bf16[256,8,128]{2,0,1:T(8,128)(2,1)S(1)}, u32[]{:S(2)}, u32[]{:S(2)}) %all-to-all-start.1) | async-done | bytes 524320 | tf_op jit(solution)/shard_map/all_to_all | solution.py:111
  34.2 3.6 %all-to-all-start = ((bf16[256,16,128]{0,2,1:T(8,128)(2,1)}), bf16[256,16,128]{0,2,1:T(8,128)(2,1)S(1)}, u32[]{:S(2)}, u32[]{:S(2)}) async-start(bf16[256,16,128]{0,2,1:T(8,128)(2,1)} %pad_maximum_fusion), calls=%async_computation | async-start | bytes 2097152 | tf_op jit(solution)/shard_map/all_to_all | solution.py:110
  38.7 25.1 %all-to-all-done = bf16[256,16,128]{0,2,1:T(8,128)(2,1)S(1)} async-done(((bf16[256,16,128]{0,2,1:T(8,128)(2,1)}), bf16[256,16,128]{0,2,1:T(8,128)(2,1)S(1)}, u32[]{:S(2)}, u32[]{:S(2)}) %all-to-all-start) | async-done | bytes 1048608 | tf_op jit(solution)/shard_map/all_to_all | solution.py:110
  64.7 3.6 %all-to-all-start.2 = ((bf16[256,8,128]{2,0,1:T(8,128)(2,1)}), bf16[256,8,128]{2,0,1:T(8,128)(2,1)S(1)}, u32[]{:S(2)}, u32[]{:S(2)}) async-start(bf16[256,8,128]{2,0,1:T(8,128)(2,1)} %bitcast.26), calls=%async_computation.2 | async-start | bytes 1048576 | tf_op jit(solution)/shard_map/all_to_all | solution.py:112
  69.0 14.0 %all-to-all-done.2 = bf16[256,8,128]{2,0,1:T(8,128)(2,1)S(1)} async-done(((bf16[256,8,128]{2,0,1:T(8,128)(2,1)}), bf16[256,8,128]{2,0,1:T(8,128)(2,1)S(1)}, u32[]{:S(2)}, u32[]{:S(2)}) %all-to-all-start.2) | async-done | bytes 524320 | tf_op jit(solution)/shard_map/all_to_all | solution.py:112
  83.0 22.7 %while.10 = (s32[]{:T(128)}, bf16[4,512,1,2,128]{4,1,0,3,2:T(8,128)(2,1)}, bf16[4,512,1,2,128]{4,1,0,3,2:T(8,128)(2,1)S(1)}, bf16[2048,1,128]{2,0,1:T(8,128)(2,1...) while((s32[]{:T(128)}, bf16[4,512,1,2,128]{4,1,0,3,2:T(8,128)(2,1)}, ...), condition=%wide.region_5.6_spmd, body=%wide.region_2.5_spmd.sunk | while | flops 1092745216 | bytes 26759752 | solution.py:65
  83.0 1.3 bitcast_reduce_fusion.2
  84.3 1.6 fusion.63
  86.0 2.7 fusion.64
  90.0 1.6 fusion.63
  91.7 2.7 fusion.64
  95.7 1.6 fusion.63
  97.3 2.7 fusion.64
  100.0 1.3 bitcast_reduce_fusion.2
  101.4 1.6 fusion.63
  103.0 2.7 fusion.64
  105.7 3.7 %copy.124 = bf16[2048,2,128]{2,1,0:T(2,128)(2,1)} copy(bf16[2048,2,128]{2,0,1:T(8,128)(2,1)} %bitcast.160) | data formatting | bytes 2097152 | tf_op jit(solution)/shard_map/reshape | solution.py:65
  109.4 3.6 %all-to-all-start.3 = ((bf16[2048,2,128]{2,1,0:T(2,128)(2,1)}), bf16[2048,2,128]{2,1,0:T(2,128)(2,1)S(1)}, u32[]{:S(2)}, u32[]{:S(2)}) async-start(bf16[2048,2,128]{2,1,0:T(2,128)(2,1)} %copy.124), calls=%async_computation.3 | async-start | bytes 2097152 | tf_op jit(solution)/shard_map/all_to_all | solution.py:115
  115.4 2.6 scatter_custom_fusion
  118.0 21.0 %all-to-all-done.3 = bf16[2048,2,128]{2,1,0:T(2,128)(2,1)S(1)} async-done(((bf16[2048,2,128]{2,1,0:T(2,128)(2,1)}), bf16[2048,2,128]{2,1,0:T(2,128)(2,1)S(1)}, u32[]{:S(2)}, u32[]{:S(2)}) %all-to-all-start.3) | async-done | bytes 1048608 | tf_op jit(solution)/shard_map/all_to_all | solution.py:115
  139.7 5.9 %fusion.33 = (f32[256]{0:T(256)S(1)}, bf16[256,2048]{1,0:T(8,128)(2,1)S(1)}) fusion(bf16[256,2048]{0,1:T(8,128)(2,1)S(1)} %bitcast.153, bf16[2048,2048]{1,0:T(8,128)(2,1)} %all-gather.2.cloned.1.call-done, bf16[1,256,2048]{2,1,0:T(8,128)(2,1)S(1)} %copy-done.2), kind=kOutput, calls=%fused_computation.39 | convolution fusion | flops 2150629120 | bytes 11535360 | tf_op jit(solution)/shard_map/dot_general | solution.py:118
  147.0 4.3 %gather_fusion = bf16[768,2048]{1,0:T(8,128)(2,1)} fusion(bf16[257,2048]{1,0:T(8,128)(2,1)S(1)} %concatenate.13, s32[1024]{0:T(1024)S(1)} %pad_clamp_fusion.1), kind=kCustom, calls=%fused_computation | custom fusion | bytes 6294528 | tf_op jit(solution)/shard_map/gather | solution.py:141
  151.3 74.8 %all_to_all.76 = bf16[32,24,2048]{2,1,0:T(8,128)(2,1)S(1)} all-to-all(bf16[32,24,2048]{2,1,0:T(8,128)(2,1)} %bitcast.150), channel_id=1, replica_groups=mesh['sp'=8,'dp'=4] {'sp','dp'}, dimensions={0} | all-to-all | bytes 6291456 | tf_op jit(solution)/shard_map/all_to_all | solution.py:143
  226.1 3.4 %fusion.23 = f32[768,1024]{1,0:T(8,128)S(1)} fusion(bf16[768,2048]{1,0:T(8,128)(2,1)S(1)} %bitcast.158, bf16[1,2048,1024]{2,1,0:T(8,128)(2,1)S(1)} %copy-done.9), kind=kOutput, calls=%fused_computation.23 | convolution fusion | flops 3221225472 | bytes 10485760 | tf_op jit(solution)/shard_map/dot_general | solution.py:72
  229.6 4.1 %multiply_convert_fusion = bf16[768,1024]{1,0:T(8,128)(2,1)S(1)} fusion(f32[768,1024]{1,0:T(8,128)S(1)} %fusion.23, bf16[768,2048]{1,0:T(8,128)(2,1)S(1)} %bitcast.159, bf16[1,2048,1024]{2,1,0:T(8,128)(2,1)S(1)} %copy-done.10), kind=kOutput, calls=%fused_computation.29 | convolution fusion | flops 3229089792 | bytes 12058624 | tf_op jit(solution)/shard_map/dot_general | solution.py:70
  233.7 4.8 %fusion.27 = bf16[768,2048]{1,0:T(8,128)(2,1)} fusion(bf16[768,1024]{1,0:T(8,128)(2,1)S(1)} %multiply_convert_fusion, bf16[1,1024,2048]{2,1,0:T(8,128)(2,1)S(1)} %copy-done.11), kind=kOutput, calls=%fused_computation.28 | convolution fusion | flops 3222798336 | bytes 8912896 | tf_op jit(solution)/shard_map/dot_general | solution.py:76
  238.5 3.9 %all-to-all-start.5 = ((bf16[32,24,2048]{2,1,0:T(8,128)(2,1)}), bf16[32,24,2048]{2,1,0:T(8,128)(2,1)S(1)}, u32[]{:S(2)}, u32[]{:S(2)}) async-start(bf16[32,24,2048]{2,1,0:T(8,128)(2,1)} %bitcast.157), calls=%async_computation.5 | async-start | bytes 6291456 | tf_op jit(solution)/shard_map/all_to_all | solution.py:148
  242.6 71.2 %all-to-all-done.5 = bf16[32,24,2048]{2,1,0:T(8,128)(2,1)S(1)} async-done(((bf16[32,24,2048]{2,1,0:T(8,128)(2,1)}), bf16[32,24,2048]{2,1,0:T(8,128)(2,1)S(1)}, u32[]{:S(2)}, u32[]{:S(2)}) %all-to-all-start.5) | async-done | bytes 3145760 | tf_op jit(solution)/shard_map/all_to_all | solution.py:148
  313.8 3.3 gather_fusion.1
  317.1 5.4 %reshape.296 = f32[256,2,2048]{2,1,0:T(2,128)} reshape(bf16[512,2048]{1,0:T(8,128)(2,1)} %gather_fusion.1) | data formatting | bytes 6291456 | tf_op jit(solution)/shard_map/convert_element_type | solution.py:150
  322.6 9.0 %multiply_reduce_fusion = f32[256,2048]{1,0:T(8,128)S(1)} fusion(f32[256,2,2048]{2,1,0:T(2,128)} %reshape.296, f32[256,2]{1,0:T(8,128)S(1)} %copy.131), kind=kLoop, calls=%fused_computation.27 | loop fusion | flops 1572864 | bytes 6293504 | tf_op jit(solution)/shard_map/reduce_sum | solution.py:151
  (79 shorter events, 19.1 us)
Async XLA Ops:
  9.8 9.9 %copy-start.3 = (bf16[1,256,2048]{2,1,0:T(8,128)(2,1)S(1)}, bf16[1,256,2048]{2,1,0:T(8,128)(2,1)}, u32[]{:S(2)}) copy-start(bf16[1,256,2048]{2,1,0:T(8,128)(2,1)} %param.16) | copy-start | bytes 3145732
  10.7 9.8 %copy-start.8 = (f32[128]{0:T(128)S(1)}, f32[128]{0:T(128)}, u32[]{:S(2)}) copy-start(f32[128]{0:T(128)} %param.19) | copy-start | bytes 1540
  12.4 21.8 %all-to-all-start.1 = ((bf16[256,8,128]{2,0,1:T(8,128)(2,1)}), bf16[256,8,128]{2,0,1:T(8,128)(2,1)S(1)}, u32[]{:S(2)}, u32[]{:S(2)}) async-start(bf16[256,8,128]{2,0,1:T(8,128)(2,1)} %bitcast.22), calls=%async_computation.1 | async-start | bytes 1048576 | tf_op jit(solution)/shard_map/all_to_all | solution.py:111
  21.2 17.3 %copy-start.4 = (bf16[1,256,512]{2,1,0:T(8,128)(2,1)S(1)}, bf16[1,256,512]{2,1,0:T(8,128)(2,1)}, u32[]{:S(2)}) copy-start(bf16[1,256,512]{2,1,0:T(8,128)(2,1)} %param.18) | copy-start | bytes 786436
  34.2 29.6 %all-to-all-start = ((bf16[256,16,128]{0,2,1:T(8,128)(2,1)}), bf16[256,16,128]{0,2,1:T(8,128)(2,1)S(1)}, u32[]{:S(2)}, u32[]{:S(2)}) async-start(bf16[256,16,128]{0,2,1:T(8,128)(2,1)} %pad_maximum_fusion), calls=%async_computation | async-start | bytes 2097152 | tf_op jit(solution)/shard_map/all_to_all | solution.py:110
  37.8 101.9 %all-gather.2.cloned.1.call-start = ((), (), s32[]{:S(2)}) async-start(), calls=%async_computation.6 | async-start | bytes 10485760 | tf_op jit(solution)/shard_map/all_gather | solution.py:120
  64.7 18.3 %all-to-all-start.2 = ((bf16[256,8,128]{2,0,1:T(8,128)(2,1)}), bf16[256,8,128]{2,0,1:T(8,128)(2,1)S(1)}, u32[]{:S(2)}, u32[]{:S(2)}) async-start(bf16[256,8,128]{2,0,1:T(8,128)(2,1)} %bitcast.26), calls=%async_computation.2 | async-start | bytes 1048576 | tf_op jit(solution)/shard_map/all_to_all | solution.py:112
  105.7 7.3 %copy-start.6 = (s32[1,256,2]{1,2,0:T(2,128)S(1)}, s32[1,256,2]{1,2,0:T(2,128)}, u32[]{:S(2)}) copy-start(s32[1,256,2]{1,2,0:T(2,128)} %param.23) | copy-start | bytes 6148
  109.4 29.6 %all-to-all-start.3 = ((bf16[2048,2,128]{2,1,0:T(2,128)(2,1)}), bf16[2048,2,128]{2,1,0:T(2,128)(2,1)S(1)}, u32[]{:S(2)}, u32[]{:S(2)}) async-start(bf16[2048,2,128]{2,1,0:T(2,128)(2,1)} %copy.124), calls=%async_computation.3 | async-start | bytes 2097152 | tf_op jit(solution)/shard_map/all_to_all | solution.py:115
  113.0 26.7 %copy-start.2 = (bf16[1,256,2048]{2,1,0:T(8,128)(2,1)S(1)}, bf16[1,256,2048]{2,1,0:T(8,128)(2,1)}, u32[]{:S(2)}) copy-start(bf16[1,256,2048]{2,1,0:T(8,128)(2,1)} %param.15) | copy-start | bytes 3145732
  139.7 6.9 %copy-start.5 = (f32[2048]{0:T(1024)S(1)}, f32[2048]{0:T(1024)}, u32[]{:S(2)}) copy-start(f32[2048]{0:T(1024)} %param.22) | copy-start | bytes 24580
  145.6 1.0 copy-start
  151.3 74.8 %copy-start.9 = (bf16[1,2048,1024]{2,1,0:T(8,128)(2,1)S(1)}, bf16[1,2048,1024]{2,1,0:T(8,128)(2,1)}, u32[]{:S(2)}) copy-start(bf16[1,2048,1024]{2,1,0:T(8,128)(2,1)} %param.26) | copy-start | bytes 12582916
  226.1 3.5 %copy-start.10 = (bf16[1,2048,1024]{2,1,0:T(8,128)(2,1)S(1)}, bf16[1,2048,1024]{2,1,0:T(8,128)(2,1)}, u32[]{:S(2)}) copy-start(bf16[1,2048,1024]{2,1,0:T(8,128)(2,1)} %param.25) | copy-start | bytes 12582916
  229.6 4.2 %copy-start.11 = (bf16[1,1024,2048]{2,1,0:T(8,128)(2,1)S(1)}, bf16[1,1024,2048]{2,1,0:T(8,128)(2,1)}, u32[]{:S(2)}) copy-start(bf16[1,1024,2048]{2,1,0:T(8,128)(2,1)} %param.27) | copy-start | bytes 12582916
  238.5 3.9 %copy-start.7 = (f32[1,256,2]{1,2,0:T(2,128)S(1)}, f32[1,256,2]{1,2,0:T(2,128)}, u32[]{:S(2)}) copy-start(f32[1,256,2]{1,2,0:T(2,128)} %param.24) | copy-start | bytes 6148
  238.5 75.3 %all-to-all-start.5 = ((bf16[32,24,2048]{2,1,0:T(8,128)(2,1)}), bf16[32,24,2048]{2,1,0:T(8,128)(2,1)S(1)}, u32[]{:S(2)}, u32[]{:S(2)}) async-start(bf16[32,24,2048]{2,1,0:T(8,128)(2,1)} %bitcast.157), calls=%async_computation.5 | async-start | bytes 6291456 | tf_op jit(solution)/shard_map/all_to_all | solution.py:148
  322.6 9.0 %copy-start.1 = (bf16[256,2048]{1,0:T(8,128)(2,1)S(1)}, bf16[256,2048]{1,0:T(8,128)(2,1)}, u32[]{:S(2)}) copy-start(bf16[256,2048]{1,0:T(8,128)(2,1)} %copy-done) | copy-start | bytes 3145732
Sparse Core Ops, SparseCore 0:
  40.2 59.6 all-gather.1
where the time goes:
time: 340 us
  waiting for transfers between devices  144 us (42%)
  blocking collectives  74.8 us (22%)
  matrix products  34.4 us (10%)
  local copies, waits for them, and re-layouts  26.8 us (8%)
  other arithmetic  23.8 us (7%)
  starting transfers between devices  22.1 us (6%)
  between operations  13.8 us (4%)
    all_to_all x1, blocking collectives, per_device(): lax.all_to_all(outgoing, ('sp', 'dp'), split_axis=0, concat_axis=0, tiled...  74.8 us
    all_to_all x1, waiting for transfers between devices, per_device(): lax.all_to_all(answered, ('sp', 'dp'), split_axis=0, concat_axis=0, tiled...  71.2 us
    all_to_all x1, waiting for transfers between devices, per_device(): lax.all_to_all(query_turned, 'sp', split_axis=1, concat_axis=0, tiled=True)  25.1 us
    all_to_all x1, waiting for transfers between devices, per_device(): lax.all_to_all(head_out, 'sp', split_axis=0, concat_axis=1, tiled=True)  21 us
    all_to_all x1, waiting for transfers between devices, per_device(): lax.all_to_all(value_heads, 'sp', split_axis=1, concat_axis=0, tiled=True)  14 us
    all_to_all x1, waiting for transfers between devices, per_device(): lax.all_to_all(key_turned, 'sp', split_axis=1, concat_axis=0, tiled=True)  11.9 us
    dot_general x4, matrix products, one_block(): jnp.einsum('kgqs,skd->qkgd', attn_weights, head_value, preferred_element_...  10.8 us
    reduce_sum x1, other arithmetic, per_device(): jnp.sum(weighted.reshape(tok_rows, top_count, model_width), axis=1)  8.96 us
  transfers between devices with their start and end apart: 6, of which 5 were waited for; matrix products, arithmetic and copies ran while one was open for 11% of the time, Pallas kernels for 0%

commit v1 on v0

--- a/solution.py
+++ b/solution.py
@@ -8,6 +8,12 @@
 THETA = 10000.0
 LIMIT = 7.0
 SLOPE = 1.702
+
+
+def mix_the_record(mine_x, named_axis, dim_i, axis_k=0):
+    low = jax.lax.psum(1, named_axis)
+    vec_out = jax.lax.all_to_all(jnp.stack(jnp.split(mine_x, low, dim_i)), named_axis, 0, 0)
+    return jnp.concatenate(vec_out, axis_k)
 
 
 def turn_half(matrix, places):
@@ -108,7 +114,7 @@
     value_heads = jnp.repeat(values[0].reshape(tok_rows, kv_heads, head_dim), repeat_count, axis=1)
     head_query, head_key, head_value = (
         lax.all_to_all(query_turned, "sp", split_axis=1, concat_axis=0, tiled=True),
-        lax.all_to_all(key_turned, "sp", split_axis=1, concat_axis=0, tiled=True),
+        mix_the_record(key_turned, "sp", 1),
         lax.all_to_all(value_heads, "sp", split_axis=1, concat_axis=0, tiled=True),
     )
     head_out = attend(head_query, head_key, head_value)

time: 340 us -> 345 us (1.015)
  local copies, waits for them, and re-layouts: 26.8 us -> 31 us
    unnamed x26 -> x33, local copies, waits for them, and re-layouts: 1.67 us -> 6.06 us
where the time goes in v1:
time: 345 us; the launch traced here: 344 us
  waiting for transfers between devices  144 us (42%)
  blocking collectives  74.8 us (22%)
  matrix products  34.4 us (10%)
  local copies, waits for them, and re-layouts  31 us (9%)
  other arithmetic  23.8 us (7%)
  starting transfers between devices  22.1 us (6%)
  between operations  13.8 us (4%)
    all_to_all x1, blocking collectives, per_device(): lax.all_to_all(outgoing, ('sp', 'dp'), split_axis=0, concat_axis=0, tiled...  74.8 us
    all_to_all x1, waiting for transfers between devices, per_device(): lax.all_to_all(answered, ('sp', 'dp'), split_axis=0, concat_axis=0, tiled...  71.2 us
    all_to_all x1, waiting for transfers between devices, per_device(): lax.all_to_all(query_turned, 'sp', split_axis=1, concat_axis=0, tiled=True)  25.1 us
    all_to_all x1, waiting for transfers between devices, per_device(): lax.all_to_all(head_out, 'sp', split_axis=0, concat_axis=1, tiled=True)  21 us
    all_to_all x1, waiting for transfers between devices, per_device(): lax.all_to_all(value_heads, 'sp', split_axis=1, concat_axis=0, tiled=True)  14 us
    all_to_all x1, waiting for transfers between devices, mix_the_record(): jax.lax.all_to_all(jnp.stack(jnp.split(mine_x, low, dim_i)), named_axis,...  11.9 us
    dot_general x4, matrix products, one_block(): jnp.einsum('kgqs,skd->qkgd', attn_weights, head_value, preferred_element_...  10.8 us
    reduce_sum x1, other arithmetic, per_device(): jnp.sum(weighted.reshape(tok_rows, top_count, model_width), axis=1)  8.96 us
  transfers between devices with their start and end apart: 6, of which 5 were waited for; matrix products, arithmetic and copies ran while one was open for 11% of the time, Pallas kernels for 0%

profile of v1, /device:TPU:0, one launch (start us, length us, event | category | flops | bytes accessed | tf_op | source)
XLA Modules:
  0.0 343.9 jit_solution(8889461181076416127)
XLA Ops:
  16.7 7.3 %all-to-all-start.1 = ((bf16[8,256,1,128]{3,1,2,0:T(8,128)(2,1)}), bf16[8,256,1,128]{3,1,2,0:T(8,128)(2,1)S(1)}, u32[]{:S(2)}, u32[]{:S(2)}) async-start(bf16[8,256,1,128]{3,1,2,0:T(8,128)(2,1)} %fusion.43), calls=%async_computation.1 | async-start | bytes 1048576 | tf_op jit(solution)/shard_map/all_to_all | solution.py:15
  26.5 11.9 %all-to-all-done.1 = bf16[8,256,1,128]{3,1,2,0:T(8,128)(2,1)S(1)} async-done(((bf16[8,256,1,128]{3,1,2,0:T(8,128)(2,1)}), bf16[8,256,1,128]{3,1,2,0:T(8,128)(2,1)S(1)}, u32[]{:S(2)}, u32[]{:S(2)}) %all-to-all-start.1) | async-done | bytes 524320 | tf_op jit(solution)/shard_map/all_to_all | solution.py:15
  38.4 3.6 %all-to-all-start = ((bf16[256,16,128]{0,2,1:T(8,128)(2,1)}), bf16[256,16,128]{0,2,1:T(8,128)(2,1)S(1)}, u32[]{:S(2)}, u32[]{:S(2)}) async-start(bf16[256,16,128]{0,2,1:T(8,128)(2,1)} %pad_maximum_fusion), calls=%async_computation | async-start | bytes 2097152 | tf_op jit(solution)/shard_map/all_to_all | solution.py:116
  42.9 25.1 %all-to-all-done = bf16[256,16,128]{0,2,1:T(8,128)(2,1)S(1)} async-done(((bf16[256,16,128]{0,2,1:T(8,128)(2,1)}), bf16[256,16,128]{0,2,1:T(8,128)(2,1)S(1)}, u32[]{:S(2)}, u32[]{:S(2)}) %all-to-all-start) | async-done | bytes 1048608 | tf_op jit(solution)/shard_map/all_to_all | solution.py:116
  68.9 3.6 %all-to-all-start.2 = ((bf16[256,8,128]{2,0,1:T(8,128)(2,1)}), bf16[256,8,128]{2,0,1:T(8,128)(2,1)S(1)}, u32[]{:S(2)}, u32[]{:S(2)}) async-start(bf16[256,8,128]{2,0,1:T(8,128)(2,1)} %bitcast.32), calls=%async_computation.2 | async-start | bytes 1048576 | tf_op jit(solution)/shard_map/all_to_all | solution.py:118
  73.3 14.0 %all-to-all-done.2 = bf16[256,8,128]{2,0,1:T(8,128)(2,1)S(1)} async-done(((bf16[256,8,128]{2,0,1:T(8,128)(2,1)}), bf16[256,8,128]{2,0,1:T(8,128)(2,1)S(1)}, u32[]{:S(2)}, u32[]{:S(2)}) %all-to-all-start.2) | async-done | bytes 524320 | tf_op jit(solution)/shard_map/all_to_all | solution.py:118
  87.3 22.7 %while.10 = (s32[]{:T(128)}, bf16[4,512,1,2,128]{4,1,0,3,2:T(8,128)(2,1)}, bf16[4,512,1,2,128]{4,1,0,3,2:T(8,128)(2,1)S(1)}, bf16[2048,1,128]{2,0,1:T(8,128)(2,1...) while((s32[]{:T(128)}, bf16[4,512,1,2,128]{4,1,0,3,2:T(8,128)(2,1)}, ...), condition=%wide.region_5.6_spmd, body=%wide.region_2.5_spmd.sunk | while | flops 1092745216 | bytes 26759752 | solution.py:71
  87.3 1.3 bitcast_reduce_fusion.2
  88.6 1.6 fusion.71
  90.2 2.7 fusion.72
  94.3 1.6 fusion.71
  95.9 2.7 fusion.72
  99.9 1.6 fusion.71
  101.6 2.7 fusion.72
  104.3 1.3 bitcast_reduce_fusion.2
  105.6 1.6 fusion.71
  107.3 2.7 fusion.72
  110.0 3.7 %copy.152 = bf16[2048,2,128]{2,1,0:T(2,128)(2,1)} copy(bf16[2048,2,128]{2,0,1:T(8,128)(2,1)} %bitcast.196) | data formatting | bytes 2097152 | tf_op jit(solution)/shard_map/reshape | solution.py:71
  113.7 3.6 %all-to-all-start.3 = ((bf16[2048,2,128]{2,1,0:T(2,128)(2,1)}), bf16[2048,2,128]{2,1,0:T(2,128)(2,1)S(1)}, u32[]{:S(2)}, u32[]{:S(2)}) async-start(bf16[2048,2,128]{2,1,0:T(2,128)(2,1)} %copy.152), calls=%async_computation.3 | async-start | bytes 2097152 | tf_op jit(solution)/shard_map/all_to_all | solution.py:121
  119.6 2.6 scatter_custom_fusion
  122.3 21.0 %all-to-all-done.3 = bf16[2048,2,128]{2,1,0:T(2,128)(2,1)S(1)} async-done(((bf16[2048,2,128]{2,1,0:T(2,128)(2,1)}), bf16[2048,2,128]{2,1,0:T(2,128)(2,1)S(1)}, u32[]{:S(2)}, u32[]{:S(2)}) %all-to-all-start.3) | async-done | bytes 1048608 | tf_op jit(solution)/shard_map/all_to_all | solution.py:121
  144.0 5.9 %fusion.33 = (f32[256]{0:T(256)S(1)}, bf16[256,2048]{1,0:T(8,128)(2,1)S(1)}) fusion(bf16[256,2048]{0,1:T(8,128)(2,1)S(1)} %bitcast.181, bf16[2048,2048]{1,0:T(8,128)(2,1)} %all-gather.2.cloned.1.call-done, bf16[1,256,2048]{2,1,0:T(8,128)(2,1)S(1)} %copy-done.2), kind=kOutput, calls=%fused_computation.39 | convolution fusion | flops 2150629120 | bytes 11535360 | tf_op jit(solution)/shard_map/dot_general | solution.py:124
  151.2 4.3 %gather_fusion = bf16[768,2048]{1,0:T(8,128)(2,1)} fusion(bf16[257,2048]{1,0:T(8,128)(2,1)S(1)} %concatenate.13, s32[1024]{0:T(1024)S(1)} %pad_clamp_fusion.1), kind=kCustom, calls=%fused_computation | custom fusion | bytes 6294528 | tf_op jit(solution)/shard_map/gather | solution.py:147
  155.5 74.8 %all_to_all.63 = bf16[32,24,2048]{2,1,0:T(8,128)(2,1)S(1)} all-to-all(bf16[32,24,2048]{2,1,0:T(8,128)(2,1)} %bitcast.178), channel_id=1, replica_groups=mesh['sp'=8,'dp'=4] {'sp','dp'}, dimensions={0} | all-to-all | bytes 6291456 | tf_op jit(solution)/shard_map/all_to_all | solution.py:149
  230.3 3.4 %fusion.23 = f32[768,1024]{1,0:T(8,128)S(1)} fusion(bf16[768,2048]{1,0:T(8,128)(2,1)S(1)} %bitcast.186, bf16[1,2048,1024]{2,1,0:T(8,128)(2,1)S(1)} %copy-done.9), kind=kOutput, calls=%fused_computation.23 | convolution fusion | flops 3221225472 | bytes 10485760 | tf_op jit(solution)/shard_map/dot_general | solution.py:78
  233.8 4.1 %multiply_convert_fusion = bf16[768,1024]{1,0:T(8,128)(2,1)S(1)} fusion(f32[768,1024]{1,0:T(8,128)S(1)} %fusion.23, bf16[768,2048]{1,0:T(8,128)(2,1)S(1)} %bitcast.187, bf16[1,2048,1024]{2,1,0:T(8,128)(2,1)S(1)} %copy-done.10), kind=kOutput, calls=%fused_computation.29 | convolution fusion | flops 3229089792 | bytes 12058624 | tf_op jit(solution)/shard_map/dot_general | solution.py:76
  238.0 4.8 %fusion.27 = bf16[768,2048]{1,0:T(8,128)(2,1)} fusion(bf16[768,1024]{1,0:T(8,128)(2,1)S(1)} %multiply_convert_fusion, bf16[1,1024,2048]{2,1,0:T(8,128)(2,1)S(1)} %copy-done.11), kind=kOutput, calls=%fused_computation.28 | convolution fusion | flops 3222798336 | bytes 8912896 | tf_op jit(solution)/shard_map/dot_general | solution.py:82
  242.8 3.9 %all-to-all-start.5 = ((bf16[32,24,2048]{2,1,0:T(8,128)(2,1)}), bf16[32,24,2048]{2,1,0:T(8,128)(2,1)S(1)}, u32[]{:S(2)}, u32[]{:S(2)}) async-start(bf16[32,24,2048]{2,1,0:T(8,128)(2,1)} %bitcast.185), calls=%async_computation.5 | async-start | bytes 6291456 | tf_op jit(solution)/shard_map/all_to_all | solution.py:154
  246.8 71.2 %all-to-all-done.5 = bf16[32,24,2048]{2,1,0:T(8,128)(2,1)S(1)} async-done(((bf16[32,24,2048]{2,1,0:T(8,128)(2,1)}), bf16[32,24,2048]{2,1,0:T(8,128)(2,1)S(1)}, u32[]{:S(2)}, u32[]{:S(2)}) %all-to-all-start.5) | async-done | bytes 3145760 | tf_op jit(solution)/shard_map/all_to_all | solution.py:154
  318.0 3.3 gather_fusion.1
  321.4 5.4 %reshape.300 = f32[256,2,2048]{2,1,0:T(2,128)} reshape(bf16[512,2048]{1,0:T(8,128)(2,1)} %gather_fusion.1) | data formatting | bytes 6291456 | tf_op jit(solution)/shard_map/convert_element_type | solution.py:156
  326.8 9.0 %multiply_reduce_fusion = f32[256,2048]{1,0:T(8,128)S(1)} fusion(f32[256,2,2048]{2,1,0:T(2,128)} %reshape.300, f32[256,2]{1,0:T(8,128)S(1)} %copy.159), kind=kLoop, calls=%fused_computation.27 | loop fusion | flops 1572864 | bytes 6293504 | tf_op jit(solution)/shard_map/reduce_sum | solution.py:157
  (87 shorter events, 23.4 us)
Async XLA Ops:
  10.7 13.3 %copy-start.3 = (bf16[1,256,2048]{2,1,0:T(8,128)(2,1)S(1)}, bf16[1,256,2048]{2,1,0:T(8,128)(2,1)}, u32[]{:S(2)}) copy-start(bf16[1,256,2048]{2,1,0:T(8,128)(2,1)} %param.16) | copy-start | bytes 3145732
  11.6 13.2 %copy-start.8 = (f32[128]{0:T(128)S(1)}, f32[128]{0:T(128)}, u32[]{:S(2)}) copy-start(f32[128]{0:T(128)} %param.19) | copy-start | bytes 1540
  16.7 21.8 %all-to-all-start.1 = ((bf16[8,256,1,128]{3,1,2,0:T(8,128)(2,1)}), bf16[8,256,1,128]{3,1,2,0:T(8,128)(2,1)S(1)}, u32[]{:S(2)}, u32[]{:S(2)}) async-start(bf16[8,256,1,128]{3,1,2,0:T(8,128)(2,1)} %fusion.43), calls=%async_computation.1 | async-start | bytes 1048576 | tf_op jit(solution)/shard_map/all_to_all | solution.py:15
  25.5 17.3 %copy-start.4 = (bf16[1,256,512]{2,1,0:T(8,128)(2,1)S(1)}, bf16[1,256,512]{2,1,0:T(8,128)(2,1)}, u32[]{:S(2)}) copy-start(bf16[1,256,512]{2,1,0:T(8,128)(2,1)} %param.18) | copy-start | bytes 786436
  38.4 29.6 %all-to-all-start = ((bf16[256,16,128]{0,2,1:T(8,128)(2,1)}), bf16[256,16,128]{0,2,1:T(8,128)(2,1)S(1)}, u32[]{:S(2)}, u32[]{:S(2)}) async-start(bf16[256,16,128]{0,2,1:T(8,128)(2,1)} %pad_maximum_fusion), calls=%async_computation | async-start | bytes 2097152 | tf_op jit(solution)/shard_map/all_to_all | solution.py:116
  42.1 101.8 %all-gather.2.cloned.1.call-start = ((), (), s32[]{:S(2)}) async-start(), calls=%async_computation.6 | async-start | bytes 10485760 | tf_op jit(solution)/shard_map/all_gather | solution.py:126
  68.9 18.3 %all-to-all-start.2 = ((bf16[256,8,128]{2,0,1:T(8,128)(2,1)}), bf16[256,8,128]{2,0,1:T(8,128)(2,1)S(1)}, u32[]{:S(2)}, u32[]{:S(2)}) async-start(bf16[256,8,128]{2,0,1:T(8,128)(2,1)} %bitcast.32), calls=%async_computation.2 | async-start | bytes 1048576 | tf_op jit(solution)/shard_map/all_to_all | solution.py:118
  110.0 7.3 %copy-start.6 = (s32[1,256,2]{1,2,0:T(2,128)S(1)}, s32[1,256,2]{1,2,0:T(2,128)}, u32[]{:S(2)}) copy-start(s32[1,256,2]{1,2,0:T(2,128)} %param.23) | copy-start | bytes 6148
  113.7 29.6 %all-to-all-start.3 = ((bf16[2048,2,128]{2,1,0:T(2,128)(2,1)}), bf16[2048,2,128]{2,1,0:T(2,128)(2,1)S(1)}, u32[]{:S(2)}, u32[]{:S(2)}) async-start(bf16[2048,2,128]{2,1,0:T(2,128)(2,1)} %copy.152), calls=%async_computation.3 | async-start | bytes 2097152 | tf_op jit(solution)/shard_map/all_to_all | solution.py:121
  117.3 26.7 %copy-start.2 = (bf16[1,256,2048]{2,1,0:T(8,128)(2,1)S(1)}, bf16[1,256,2048]{2,1,0:T(8,128)(2,1)}, u32[]{:S(2)}) copy-start(bf16[1,256,2048]{2,1,0:T(8,128)(2,1)} %param.15) | copy-start | bytes 3145732
  143.9 6.9 %copy-start.5 = (f32[2048]{0:T(1024)S(1)}, f32[2048]{0:T(1024)}, u32[]{:S(2)}) copy-start(f32[2048]{0:T(1024)} %param.22) | copy-start | bytes 24580
  149.8 1.0 copy-start
  155.5 74.8 %copy-start.9 = (bf16[1,2048,1024]{2,1,0:T(8,128)(2,1)S(1)}, bf16[1,2048,1024]{2,1,0:T(8,128)(2,1)}, u32[]{:S(2)}) copy-start(bf16[1,2048,1024]{2,1,0:T(8,128)(2,1)} %param.26) | copy-start | bytes 12582916
  230.3 3.5 %copy-start.10 = (bf16[1,2048,1024]{2,1,0:T(8,128)(2,1)S(1)}, bf16[1,2048,1024]{2,1,0:T(8,128)(2,1)}, u32[]{:S(2)}) copy-start(bf16[1,2048,1024]{2,1,0:T(8,128)(2,1)} %param.25) | copy-start | bytes 12582916
  233.8 4.2 %copy-start.11 = (bf16[1,1024,2048]{2,1,0:T(8,128)(2,1)S(1)}, bf16[1,1024,2048]{2,1,0:T(8,128)(2,1)}, u32[]{:S(2)}) copy-start(bf16[1,1024,2048]{2,1,0:T(8,128)(2,1)} %param.27) | copy-start | bytes 12582916
  242.8 3.9 %copy-start.7 = (f32[1,256,2]{1,2,0:T(2,128)S(1)}, f32[1,256,2]{1,2,0:T(2,128)}, u32[]{:S(2)}) copy-start(f32[1,256,2]{1,2,0:T(2,128)} %param.24) | copy-start | bytes 6148
  242.8 75.3 %all-to-all-start.5 = ((bf16[32,24,2048]{2,1,0:T(8,128)(2,1)}), bf16[32,24,2048]{2,1,0:T(8,128)(2,1)S(1)}, u32[]{:S(2)}, u32[]{:S(2)}) async-start(bf16[32,24,2048]{2,1,0:T(8,128)(2,1)} %bitcast.185), calls=%async_computation.5 | async-start | bytes 6291456 | tf_op jit(solution)/shard_map/all_to_all | solution.py:154
  326.8 9.0 %copy-start.1 = (bf16[256,2048]{1,0:T(8,128)(2,1)S(1)}, bf16[256,2048]{1,0:T(8,128)(2,1)}, u32[]{:S(2)}) copy-start(bf16[256,2048]{1,0:T(8,128)(2,1)} %copy-done) | copy-start | bytes 3145732
Sparse Core Ops, SparseCore 0:
  44.4 59.6 all-gather.1
